TPU v7x, 32 devices: a whole 2x2x4 slice. The times are simulated.
32 devices in a mesh: dp: 4 (over y, x), kv: 4 (over z), tp: 2 (over core).
Axes of the slice: x: 2, y: 2, z: 4, core: 2. Of those that a mesh axis runs over, the one named last changes fastest.
Arguments:
- tokens: bfloat16 [4, 3072, 2048], P('dp', 'kv'), may hold values from -60 to 60
- query_weight: bfloat16 [2048, 1024], P(None, 'tp'), may hold values from -0.125 to 0.125
- key_weight: bfloat16 [2048, 256], P(None, 'tp'), may hold values from -0.125 to 0.125
- value_weight: bfloat16 [2048, 256], P(None, 'tp'), may hold values from -0.125 to 0.125
- out_weight: bfloat16 [1024, 2048], P('tp'), may hold values from -3 to 3
- norm_gain: float32 [2048], P('tp'), may hold values from 0.1 to 1.9
- chosen_owner: int32 [4, 24, 4], P('dp'), may hold values from -1 to 3, as said below
- chosen_part: int32 [4, 24, 4], P('dp'), may hold values from 0 to 11, as said below
Outputs:
- attended: bfloat16 [4, 3072, 2048], P('dp', 'kv', 'tp')
Inputs may be any that keep to these rules, and one draw needn't show every extreme that they name: `chosen_owner`: within a row the indices other than -1 are different. Every named key block lies wholly before its query block's first position. Among the 6 rows of one index of kv, no index is named by more than 6 rows. `chosen_part`: 0 where the owner is -1.
All inputs are finite; a program needn't handle non-finite values.
Results may differ from a plain program's by a relative error of at most 0.014.
The roundings to bfloat16 on the way count: a program that leaves them out, or rounds other values in their place, can miss the bound.
Values may be sent and summed in bfloat16 or wider, within the bound.
A program may use at most 128 MiB of HBM per device.

v0:
```python
import jax
import jax.numpy as jnp
from jax import lax
from jax.sharding import PartitionSpec as P

D = 2048
HEAD_DIM = 64
QUERY_BLOCK = 128
KEY_BLOCK = 64
rope_base = 10000.0
norm_eps = 1e-06


def rotate(head_rows, positions):
    half_dim = head_rows.shape[-1] // 2
    frequency = rope_base ** (-jnp.arange(half_dim, dtype=jnp.float32) / half_dim)
    angles = positions.astype(jnp.float32)[:, None] * frequency
    cosine = jnp.cos(angles)[:, None, :]
    sine_part = jnp.sin(angles)[:, None, :]
    first_half = head_rows[..., :half_dim]
    second_half = head_rows[..., half_dim:]
    return jnp.concatenate(
        [
            first_half * cosine - second_half * sine_part,
            second_half * cosine + first_half * sine_part,
        ],
        axis=-1,
    )


def rank_within(flat_ids):
    entry_count = flat_ids.shape[0]
    same_owner = flat_ids[:, None] == flat_ids[None, :]
    earlier = jnp.arange(entry_count)[None, :] < jnp.arange(entry_count)[:, None]
    return jnp.sum(jnp.logical_and(same_owner, earlier), axis=1)


def body(
    tokens, query_weight, key_weight, value_weight, out_weight, norm_gain, chosen_owner, chosen_part
):
    row_data = tokens[0]
    tok_count = row_data.shape[0]
    devices = lax.axis_size("kv")
    my_index = lax.axis_index("kv")
    positions = my_index * tok_count + jnp.arange(tok_count, dtype=jnp.int32)
    heads_here = query_weight.shape[1] // HEAD_DIM
    kv_here = key_weight.shape[1] // HEAD_DIM
    group_size = heads_here // kv_here
    kv_width = kv_here * HEAD_DIM
    queries = rotate(
        jnp.dot(row_data, query_weight, preferred_element_type=jnp.float32).reshape(
            tok_count, heads_here, HEAD_DIM
        ),
        positions,
    ).astype(jnp.bfloat16)
    key_rows = (
        rotate(
            jnp.dot(row_data, key_weight, preferred_element_type=jnp.float32).reshape(
                tok_count, kv_here, HEAD_DIM
            ),
            positions,
        )
        .astype(jnp.bfloat16)
        .reshape(tok_count, kv_width)
    )
    value_rows = jnp.dot(row_data, value_weight, preferred_element_type=jnp.float32).astype(
        jnp.bfloat16
    )
    per_device = tok_count // KEY_BLOCK
    qblocks = tok_count // QUERY_BLOCK
    chosen_count = chosen_owner.shape[2]
    owner_ids = chosen_owner[0]
    part_ids = chosen_part[0]
    mine_owner = lax.dynamic_slice_in_dim(owner_ids, my_index * qblocks, qblocks, 0).reshape(
        qblocks * chosen_count
    )
    mine_valid = mine_owner >= 0
    key_blocks = key_rows.reshape(per_device, KEY_BLOCK, kv_width)
    value_blocks = value_rows.reshape(per_device, KEY_BLOCK, kv_width)
    every_owner = owner_ids.reshape(devices, qblocks * chosen_count)
    every_part = part_ids.reshape(devices, qblocks * chosen_count)
    every_rank = jax.vmap(rank_within)(every_owner)
    slot_ids = jnp.arange(qblocks, dtype=jnp.int32)
    picked_mask = jnp.logical_and(
        (every_owner == my_index)[:, None, :], every_rank[:, None, :] == slot_ids[None, :, None]
    )
    wanted = jnp.sum(jnp.where(picked_mask, every_part[:, None, :], 0), axis=2)
    send_keys = key_blocks[wanted]
    send_values = value_blocks[wanted]
    got_keys, got_values = (
        lax.all_to_all(send_keys, "kv", split_axis=0, concat_axis=0, tiled=True),
        lax.all_to_all(send_values, "kv", split_axis=0, concat_axis=0, tiled=True),
    )
    slot_index = jnp.where(mine_valid, mine_owner * qblocks + rank_within(mine_owner), 0)
    picked_keys = got_keys.reshape(devices * qblocks, KEY_BLOCK, kv_width)[slot_index]
    picked_values = got_values.reshape(devices * qblocks, KEY_BLOCK, kv_width)[slot_index]
    block_queries = queries.reshape(qblocks, QUERY_BLOCK, kv_here, group_size, HEAD_DIM)
    chosen_keys = picked_keys.reshape(qblocks, chosen_count * KEY_BLOCK, kv_here, HEAD_DIM)
    chosen_values = picked_values.reshape(qblocks, chosen_count * KEY_BLOCK, kv_here, HEAD_DIM)
    all_keys = jnp.concatenate(
        [chosen_keys, key_rows.reshape(qblocks, QUERY_BLOCK, kv_here, HEAD_DIM)], axis=1
    )
    all_values = jnp.concatenate(
        [chosen_values, value_rows.reshape(qblocks, QUERY_BLOCK, kv_here, HEAD_DIM)], axis=1
    )
    key_valid = jnp.broadcast_to(
        mine_valid.reshape(qblocks, chosen_count, 1), (qblocks, chosen_count, KEY_BLOCK)
    ).reshape(qblocks, chosen_count * KEY_BLOCK)
    far_mask = jnp.broadcast_to(
        key_valid[:, None, :], (qblocks, QUERY_BLOCK, chosen_count * KEY_BLOCK)
    )
    lower_mask = jnp.broadcast_to(
        (jnp.arange(QUERY_BLOCK)[:, None] >= jnp.arange(QUERY_BLOCK)[None, :])[None],
        (qblocks, QUERY_BLOCK, QUERY_BLOCK),
    )
    full_mask = jnp.concatenate([far_mask, lower_mask], axis=2)
    scores = jnp.einsum(
        "bqngd,bknd->bngqk", block_queries, all_keys, preferred_element_type=jnp.float32
    ) * HEAD_DIM ** (-0.5)
    scores = jnp.where(full_mask[:, None, None], scores, -jnp.inf)
    row_max = jnp.max(scores, axis=-1, keepdims=True)
    weights = jnp.exp(scores - row_max)
    weights = (weights / jnp.sum(weights, axis=-1, keepdims=True)).astype(jnp.bfloat16)
    mixed_rows = (
        jnp.einsum("bngqk,bknd->bqngd", weights, all_values, preferred_element_type=jnp.float32)
        .astype(jnp.bfloat16)
        .reshape(tok_count, heads_here * HEAD_DIM)
    )
    terms = jnp.dot(mixed_rows, out_weight, preferred_element_type=jnp.float32)
    projected = lax.psum_scatter(
        terms.astype(jnp.bfloat16), "tp", scatter_dimension=1, tiled=True
    ).astype(jnp.float32)
    row_total = lax.psum(jnp.sum(projected * projected, axis=1), "tp")
    scale_rows = lax.rsqrt(row_total / D + norm_eps)
    result = (projected * scale_rows[:, None] * norm_gain[None, :]).astype(jnp.bfloat16)
    return result[None]


def solution(mesh):
    placed = (
        P("dp", "kv", None),
        P(None, "tp"),
        P(None, "tp"),
        P(None, "tp"),
        P("tp", None),
        P("tp"),
        P("dp", None, None),
        P("dp", None, None),
    )
    return jax.shard_map(
        body, mesh=mesh, in_specs=placed, out_specs=P("dp", "kv", "tp"), check_vma=False
    )
```

profile of v0, /device:TPU:0, one launch (start us, length us, event | category | flops | bytes accessed | tf_op | source)
XLA Modules:
  0.0 117.1 jit_solution(5359210719336470150)
XLA Ops:
  7.2 2.3 %copy.52 = bf16[2048,128]{0,1:T(8,128)(2,1)} copy(bf16[2048,128]{1,0:T(8,128)(2,1)} %param.10) | data formatting | bytes 1048576 | tf_op args[2]
  9.9 2.2 %fusion.13 = f32[768,2,64]{0,2,1:T(8,128)S(1)} fusion(bf16[2,64,2048]{2,1,0:T(8,128)(2,1)} %bitcast.97, bf16[1,768,2048]{2,1,0:T(8,128)(2,1)S(1)} %copy-done), kind=kOutput, calls=%fused_computation.22 | convolution fusion | flops 402653184 | bytes 4063232 | tf_op jit(solution)/shard_map/dot_general | solution.py:58
  15.9 1.5 %convert_reduce_fusion = s32[4,24]{1,0:T(4,128)} fusion(s32[4,24]{1,0:T(4,128)S(1)} %reshape_squeeze.3, pred[24,24]{1,0:T(8,128)(4,1)} %iota_compare_fusion.2), kind=kLoop, calls=%fused_computation.49 | loop fusion | flops 9120 | bytes 1344 | tf_op jit(solution)/shard_map/vmap()/reduce_sum | solution.py:35
  20.7 6.3 %all-to-all-start.1 = ((bf16[4,6,64,128]{3,2,1,0:T(8,128)(2,1)}), bf16[4,6,64,128]{3,2,1,0:T(8,128)(2,1)}, u32[]{:S(2)}, u32[]{:S(2)}) async-start(bf16[4,6,64,128]{3,2,1,0:T(8,128)(2,1)} %bitcast.95), calls=%async_computation.1 | async-start | bytes 786432 | tf_op jit(solution)/shard_map/all_to_all | solution.py:91
  28.9 4.0 %copy.57 = bf16[2048,512]{0,1:T(8,128)(2,1)} copy(bf16[2048,512]{1,0:T(8,128)(2,1)} %param.9) | data formatting | bytes 4194304 | tf_op args[1]
  32.9 4.6 %fusion.11 = f32[768,8,64]{0,2,1:T(8,128)} fusion(bf16[8,64,2048]{2,1,0:T(8,128)(2,1)} %bitcast.92, bf16[1,768,2048]{2,1,0:T(8,128)(2,1)S(1)} %copy-done), kind=kOutput, calls=%fused_computation.20 | convolution fusion | flops 1610612736 | bytes 6815744 | tf_op jit(solution)/shard_map/dot_general | solution.py:51
  40.6 2.5 %subtract_convert_fusion = (bf16[768,8,32]{0,2,1:T(8,128)(2,1)}, bf16[768,8,32]{0,2,1:T(8,128)(2,1)}) fusion(f32[768,8,64]{0,2,1:T(8,128)} %fusion.11, f32[768,32]{0,1:T(8,128)S(1)} %get-tuple-element.12, f32[768,32]{0,1:T(8,128)S(1)} %get-tuple-element.11), kind=kLoop, calls=%fused_computation.35 | loop fusion | flops 1572864 | bytes 2555904 | tf_op jit(solution)/shard_map/convert.3
  43.0 5.1 %all-to-all-start = ((bf16[4,6,64,128]{3,2,1,0:T(8,128)(2,1)}), bf16[4,6,64,128]{3,2,1,0:T(8,128)(2,1)}, u32[]{:S(2)}, u32[]{:S(2)}) async-start(bf16[4,6,64,128]{3,2,1,0:T(8,128)(2,1)} %bitcast.94), calls=%async_computation | async-start | bytes 786432 | tf_op jit(solution)/shard_map/all_to_all | solution.py:92
  50.0 2.2 %concatenate.37 = bf16[6,128,2,4,32]{1,0,4,3,2:T(8,128)(2,1)} reshape(bf16[768,8,32]{0,2,1:T(8,128)(2,1)} %get-tuple-element.7) | data formatting | bytes 786432 | tf_op jit(solution)/shard_map/concatenate | solution.py:22
  52.2 1.9 %copy.58 = bf16[6,128,2,4,32]{1,4,3,2,0:T(8,128)(2,1)} copy(bf16[6,128,2,4,32]{1,0,4,3,2:T(8,128)(2,1)} %concatenate.37) | data formatting | bytes 786432 | tf_op jit(solution)/shard_map/concatenate | solution.py:22
  54.1 2.2 %concatenate.38 = bf16[6,128,2,4,32]{1,0,4,3,2:T(8,128)(2,1)} reshape(bf16[768,8,32]{0,2,1:T(8,128)(2,1)} %get-tuple-element.8) | data formatting | bytes 786432 | tf_op jit(solution)/shard_map/concatenate | solution.py:22
  56.3 1.9 %copy.59 = bf16[6,128,2,4,32]{1,4,3,2,0:T(8,128)(2,1)} copy(bf16[6,128,2,4,32]{1,0,4,3,2:T(8,128)(2,1)} %concatenate.38) | data formatting | bytes 786432 | tf_op jit(solution)/shard_map/concatenate | solution.py:22
  60.2 1.7 %copy_bitcast_fusion = (bf16[6,128,2,32]{1,3,2,0:T(8,128)(2,1)}, bf16[6,128,2,32]{1,3,2,0:T(8,128)(2,1)}) fusion(bf16[768,2,32]{0,2,1:T(8,128)(2,1)} %copy-done.2, bf16[768,2,32]{0,2,1:T(8,128)(2,1)} %copy-done.3), kind=kLoop, calls=%fused_computation.46 | loop fusion | bytes 393216 | tf_op jit(solution)/shard_map/concatenate | solution.py:22
  61.9 1.6 %gather_fusion.3 = bf16[24,64,128]{2,1,0:T(8,128)(2,1)S(1)} fusion(bf16[24,64,128]{2,1,0:T(8,128)(2,1)} %bitcast.14, s32[1024]{0:T(1024)S(1)} %pad_clamp_fusion), kind=kCustom, calls=%fused_computation.3 | custom fusion | bytes 786528 | tf_op jit(solution)/shard_map/gather | solution.py:95
  64.8 2.9 %copy.56 = bf16[6,256,2,64]{1,3,2,0:T(8,128)(2,1)} copy(bf16[6,256,2,64]{3,2,1,0:T(2,128)(2,1)} %reshape.208) | data formatting | bytes 786432 | tf_op jit(solution)/shard_map/reshape | solution.py:98
  67.6 1.6 %gather_fusion.1 = bf16[24,64,128]{2,1,0:T(8,128)(2,1)S(1)} fusion(bf16[24,64,128]{2,1,0:T(8,128)(2,1)} %bitcast.4, s32[1024]{0:T(1024)S(1)} %pad_clamp_fusion), kind=kCustom, calls=%fused_computation.1 | custom fusion | bytes 786528 | tf_op jit(solution)/shard_map/gather | solution.py:96
  70.5 2.2 %copy.49 = bf16[6,256,2,64]{1,3,2,0:T(8,128)(2,1)S(1)} copy(bf16[6,256,2,64]{3,2,1,0:T(2,128)(2,1)} %reshape.205) | data formatting | bytes 786432 | tf_op jit(solution)/shard_map/reshape | solution.py:99
  72.7 8.9 %fusion.38 = (f32[6,2,4,128]{3,2,1,0:T(4,128)}, f32[6,2,4,128,384]{3,4,2,1,0:T(8,128)}) fusion(pred[6,128,384]{1,2,0:T(8,128)(4,1)} %pad_add_fusion, bf16[6,128,2,4,32]{1,4,3,2,0:T(8,128)(2,1)} %copy.59, bf16[6,128,2,4,32]{1,4,3,2,0:T(8,128)(2,1)} %copy.58, bf16[6,128,2,32]{1,3,2,0:T(8,128)(2,1)} %get-tuple-element.15, ...), kind=kOutput, calls=%fused_computation.74 | convolution fusion | flops 314769792 | bytes 11132928 | tf_op jit(solution)/shard_map/sub | solution.py:122
  81.5 4.8 %fusion.19 = bf16[6,128,2,4,64]{1,4,3,2,0:T(8,128)(2,1)S(1)} fusion(f32[6,2,4,128,384]{3,4,2,1,0:T(8,128)} %get-tuple-element.14, f32[6,2,4,128]{3,2,1,0:T(4,128)} %get-tuple-element.13, bf16[6,128,2,64]{1,3,2,0:T(8,128)(2,1)} %copy.50, bf16[6,256,2,64]{1,3,2,0:T(8,128)(2,1)S(1)} %copy.49), kind=kOutput, calls=%fused_computation.28 | convolution fusion | flops 308281344 | bytes 10838016 | tf_op jit(solution)/shard_map/bngqk,bknd->bqngd/dot_general | solution.py:125
  86.9 3.5 %convolution_convert_fusion = bf16[768,2048]{1,0:T(8,128)(2,1)} fusion(bf16[512,2048]{1,0:T(8,128)(2,1)S(1)} %copy-done.7, bf16[64,8,6,128]{3,2,1,0:T(8,128)(2,1)S(1)} %bitcast.96), kind=kOutput, calls=%fused_computation.16 | convolution fusion | flops 1612185600 | bytes 6029312 | tf_op jit(solution)/shard_map/dot_general | solution.py:129
  90.4 12.6 %reduce-scatter.2.cloned.1.call-done = bf16[768,1024]{1,0:T(8,128)(2,1)} async-done(((bf16[768,2048]{1,0:T(8,128)(2,1)}), bf16[768,1024]{1,0:T(8,128)(2,1)}) %reduce-scatter.2.cloned.1.call-update) | async-done | bytes 1572880 | tf_op jit(solution)/shard_map/reduce_scatter | solution.py:130
  103.0 1.8 %fusion.8 = f32[768]{0:T(1024)S(1)} fusion(bf16[768,1024]{1,0:T(8,128)(2,1)} %reduce-scatter.2.cloned.1.call-done), kind=kLoop, calls=%fused_computation.17 | loop fusion | flops 2358528 | bytes 1575936 | tf_op jit(solution)/shard_map/reduce_sum | solution.py:133
  104.8 2.5 %psum.7 = f32[768]{0:T(1024)S(1)} all-reduce(f32[768]{0:T(1024)S(1)} %fusion.8), channel_id=1, replica_groups=mesh['dp'=4,'kv'=4,'tp'=2] {'tp'}, use_global_device_ids=true, to_apply=%region_7.8 | all-reduce | flops 768 | bytes 6144 | tf_op jit(solution)/shard_map/psum | solution.py:133
  107.3 3.0 %fusion.17 = bf16[1,768,1024]{2,1,0:T(8,128)(2,1)} fusion(bf16[768,1024]{1,0:T(8,128)(2,1)} %reduce-scatter.2.cloned.1.call-done, f32[1024]{0:T(1024)S(1)} %copy-done.5, f32[768]{0:T(1024)S(1)} %add_rsqrt_fusion), kind=kLoop, calls=%fused_computation.26 | loop fusion | flops 3145728 | bytes 3152896 | tf_op jit(solution)/shard_map/broadcast_in_dim | solution.py:136
  (68 shorter events, 19.9 us)
Async XLA Ops:
  6.5 3.4 %copy-start = (bf16[1,768,2048]{2,1,0:T(8,128)(2,1)S(1)}, bf16[1,768,2048]{2,1,0:T(8,128)(2,1)}, u32[]{:S(2)}) copy-start(bf16[1,768,2048]{2,1,0:T(8,128)(2,1)} %param.8) | copy-start | bytes 9437188
  9.9 5.3 %copy-start.4 = (s32[1,24,4]{1,2,0:T(4,128)S(1)}, s32[1,24,4]{1,2,0:T(4,128)}, u32[]{:S(2)}) copy-start(s32[1,24,4]{1,2,0:T(4,128)} %param.14) | copy-start | bytes 1156
  12.2 0.6 copy-start.2
  12.2 0.7 copy-start.3
  20.7 22.3 %all-to-all-start.1 = ((bf16[4,6,64,128]{3,2,1,0:T(8,128)(2,1)}), bf16[4,6,64,128]{3,2,1,0:T(8,128)(2,1)}, u32[]{:S(2)}, u32[]{:S(2)}) async-start(bf16[4,6,64,128]{3,2,1,0:T(8,128)(2,1)} %bitcast.95), calls=%async_computation.1 | async-start | bytes 786432 | tf_op jit(solution)/shard_map/all_to_all | solution.py:91
  32.9 4.6 %copy-start.8 = (bf16[2048,128]{1,0:T(8,128)(2,1)S(1)}, bf16[2048,128]{1,0:T(8,128)(2,1)}, u32[]{:S(2)}) copy-start(bf16[2048,128]{1,0:T(8,128)(2,1)} %param.11) | copy-start | bytes 1572868
  40.6 9.2 %copy-start.6 = (pred[6,4]{0,1:T(4,128)(4,1)S(1)}, pred[6,4]{0,1:T(4,128)(4,1)}, u32[]{:S(2)}) copy-start(pred[6,4]{0,1:T(4,128)(4,1)} %fusion.43) | copy-start | bytes 76
  43.0 24.6 %all-to-all-start = ((bf16[4,6,64,128]{3,2,1,0:T(8,128)(2,1)}), bf16[4,6,64,128]{3,2,1,0:T(8,128)(2,1)}, u32[]{:S(2)}, u32[]{:S(2)}) async-start(bf16[4,6,64,128]{3,2,1,0:T(8,128)(2,1)} %bitcast.94), calls=%async_computation | async-start | bytes 786432 | tf_op jit(solution)/shard_map/all_to_all | solution.py:92
  48.1 54.9 %reduce-scatter.2.cloned.1.call-start = ((), (), s32[]{:S(2)}) async-start(), calls=%async_computation.3 | async-start | bytes 4718592 | tf_op jit(solution)/shard_map/reduce_scatter | solution.py:130
  49.7 8.5 %copy-start.1 = (bf16[6,128,2,64]{3,2,1,0:T(2,128)(2,1)S(1)}, bf16[6,128,2,64]{3,2,1,0:T(2,128)(2,1)}, u32[]{:S(2)}) copy-start(bf16[6,128,2,64]{3,2,1,0:T(2,128)(2,1)} %reshape.247) | copy-start | bytes 589828
  81.5 5.4 %copy-start.7 = (bf16[512,2048]{1,0:T(8,128)(2,1)S(1)}, bf16[512,2048]{1,0:T(8,128)(2,1)}, u32[]{:S(2)}) copy-start(bf16[512,2048]{1,0:T(8,128)(2,1)} %param.12) | copy-start | bytes 6291460
  90.4 16.9 %copy-start.5 = (f32[1024]{0:T(1024)S(1)}, f32[1024]{0:T(1024)}, u32[]{:S(2)}) copy-start(f32[1024]{0:T(1024)} %param.13) | copy-start | bytes 12292
Sparse Core Ops, SparseCore 0:
  90.5 12.3 reduce-scatter.1
where the time goes:
time: 118 us; the launch traced here: 117 us
  local copies, waits for them, and re-layouts  37.9 us (32%)
  matrix products  25 us (21%)
  other arithmetic  14.1 us (12%)
  between operations  13.6 us (12%)
  waiting for transfers between devices  12.6 us (11%)
  starting transfers between devices  11.4 us (10%)
  blocking collectives  2.47 us (2%)
    reduce_scatter x1, waiting for transfers between devices, body(): lax.psum_scatter(terms.astype(jnp.bfloat16), 'tp', scatter_dimension=1, t...  12.6 us
    concatenate x6, local copies, waits for them, and re-layouts, rotate(): jnp.concatenate([first_half * cosine - second_half * sine_part, second_ha...  11 us
    sub x1, matrix products, body(): weights = jnp.exp(scores - row_max)  8.85 us
    unnamed x22, local copies, waits for them, and re-layouts  7.87 us
    all_to_all x1, starting transfers between devices, body(): lax.all_to_all(send_keys, 'kv', split_axis=0, concat_axis=0, tiled=True)  6.35 us
    all_to_all x1, starting transfers between devices, body(): lax.all_to_all(send_values, 'kv', split_axis=0, concat_axis=0, tiled=True)  5.1 us
    dot_general x1, matrix products, body(): jnp.einsum('bngqk,bknd->bqngd', weights, all_values, preferred_element_ty...  4.79 us
    dot_general x1, matrix products, body(): jnp.dot(row_data, query_weight, preferred_element_type=jnp.float32)  4.62 us
  transfers between devices with their start and end apart: 3, of which 1 were waited for; matrix products, arithmetic and copies ran while one was open for 30% of the time, Pallas kernels for 0%

commit v1 on v0

--- a/solution.py
+++ b/solution.py
@@ -9,6 +9,29 @@
 KEY_BLOCK = 64
 rope_base = 10000.0
 norm_eps = 1e-06
+
+
+def split_up(x, dim, count):
+    dims = x.shape
+    pieces = x.reshape(*dims[:dim], count, dims[dim] // count, *dims[dim + 1 :])
+    return jnp.moveaxis(pieces, dim, 0)
+
+
+def joined_along(tiles, dim):
+    shape = list(tiles.shape[1:])
+    shape[dim] *= tiles.shape[0]
+    return jnp.moveaxis(tiles, 0, dim).reshape(shape)
+
+
+def sent_to_each(x, axis, split_dim, concat_dim):
+    peers, index = (lax.axis_size(axis), lax.axis_index(axis))
+    parts = split_up(x, split_dim, peers)
+    outs = [parts[index]]
+    for step in range(1, peers):
+        sent = parts[(index + step) % peers]
+        outs.append(lax.ppermute(sent, axis, [(i, (i + step) % peers) for i in range(peers)]))
+    parts = jnp.stack(outs)[(index - jnp.arange(peers)) % peers]
+    return joined_along(parts, concat_dim)
 
 
 def rotate(head_rows, positions):
@@ -88,7 +111,7 @@
     send_keys = key_blocks[wanted]
     send_values = value_blocks[wanted]
     got_keys, got_values = (
-        lax.all_to_all(send_keys, "kv", split_axis=0, concat_axis=0, tiled=True),
+        sent_to_each(send_keys, "kv", 0, 0),
         lax.all_to_all(send_values, "kv", split_axis=0, concat_axis=0, tiled=True),
     )
     slot_index = jnp.where(mine_valid, mine_owner * qblocks + rank_within(mine_owner), 0)

time: 118 us -> 125 us (1.059)
  local copies, waits for them, and re-layouts: 37.9 us -> 43.2 us
  other arithmetic: 14.1 us -> 16 us
    ppermute x0 -> x3, starting transfers between devices: none -> 6.99 us  [sent_to_each(): lax.ppermute(sent, axis, [(i, (i + step) % peers) for i in range(peers)])]
    all_to_all x1 -> x0, starting transfers between devices: 6.35 us -> none  [body(): lax.all_to_all(send_keys, 'kv', split_axis=0, concat_axis=0, tiled=True)]
    concatenate x6, local copies, waits for them, and re-layouts: 11 us -> 9.05 us  [rotate(): jnp.concatenate([first_half * cosine - second_half * sine_part, second_ha...]
    dynamic_slice x0 -> x1, local copies, waits for them, and re-layouts: none -> 1.8 us  [sent_to_each(): outs = [parts[index]]]
    gather x0 -> x1, local copies, waits for them, and re-layouts: none -> 1.46 us  [sent_to_each(): parts = jnp.stack(outs)[(index - jnp.arange(peers)) % peers]]
    gather x0 -> x1, other arithmetic: none -> 1.25 us  [sent_to_each(): parts = jnp.stack(outs)[(index - jnp.arange(peers)) % peers]]
    another operation x2 -> x3, other arithmetic: 2.51 us -> 2.09 us  [the longest x1 1.09 us: sent_to_each(): parts = jnp.stack(outs)[(index - jnp.arange(peers)) % peers]]
  transfers between devices with their start and end apart: 3 -> 5, of which waited for: 1 -> 1; matrix products, arithmetic and copies ran while one was open for 30% -> 40% of each run, Pallas kernels for 0% -> 0%
where the time goes in v1:
time: 125 us; the launch traced here: 124 us
  local copies, waits for them, and re-layouts  43.2 us (35%)
  matrix products  24.8 us (20%)
  other arithmetic  16 us (13%)
  between operations  13.7 us (11%)
  waiting for transfers between devices  12.3 us (10%)
  starting transfers between devices  11.3 us (9%)
  blocking collectives  2.47 us (2%)
    reduce_scatter x1, waiting for transfers between devices, body(): lax.psum_scatter(terms.astype(jnp.bfloat16), 'tp', scatter_dimension=1, t...  12.3 us
    concatenate x6, local copies, waits for them, and re-layouts, rotate(): jnp.concatenate([first_half * cosine - second_half * sine_part, second_ha...  9.05 us
    sub x1, matrix products, body(): weights = jnp.exp(scores - row_max)  8.71 us
    unnamed x22, local copies, waits for them, and re-layouts  7.19 us
    ppermute x3, starting transfers between devices, sent_to_each(): lax.ppermute(sent, axis, [(i, (i + step) % peers) for i in range(peers)])  6.99 us
    dot_general x1, matrix products, body(): jnp.einsum('bngqk,bknd->bqngd', weights, all_values, preferred_element_ty...  4.8 us
    all_to_all x1, starting transfers between devices, body(): lax.all_to_all(send_values, 'kv', split_axis=0, concat_axis=0, tiled=True)  4.12 us
    dot_general x1, matrix products, body(): terms = jnp.dot(mixed_rows, out_weight, preferred_element_type=jnp.float32)  3.51 us
  transfers between devices with their start and end apart: 5, of which 1 were waited for; matrix products, arithmetic and copies ran while one was open for 40% of the time, Pallas kernels for 0%

profile of v1, /device:TPU:0, one launch (start us, length us, event | category | flops | bytes accessed | tf_op | source)
XLA Modules:
  0.0 123.7 jit_solution(12304263627782367495)
XLA Ops:
  7.2 2.3 %copy.54 = bf16[2048,128]{0,1:T(8,128)(2,1)} copy(bf16[2048,128]{1,0:T(8,128)(2,1)} %param.10) | data formatting | bytes 1048576 | tf_op args[2]
  10.0 2.3 %fusion.13 = f32[768,2,64]{0,2,1:T(8,128)S(1)} fusion(bf16[2,64,2048]{2,1,0:T(8,128)(2,1)} %bitcast.107, bf16[1,768,2048]{2,1,0:T(8,128)(2,1)S(1)} %copy-done), kind=kOutput, calls=%fused_computation.23 | convolution fusion | flops 402653184 | bytes 4063232 | tf_op jit(solution)/shard_map/dot_general | solution.py:81
  20.1 1.8 %dynamic-slice_bitcast_fusion = (bf16[1,1,6,64,128]{4,3,2,1,0:T(8,128)(2,1)}, bf16[1,6,64,128]{3,2,1,0:T(8,128)(2,1)}, bf16[1,6,64,128]{3,2,1,0:T(8,128)(2,1)}, bf16[1,6,64,128]{3,2,1,0:T(8,128)(2,1)}) fusion(bf16[4,6,64,128]{3,2,1,0:T(8,128)(2,1)} %bitcast.104, s32[]{:T(128)S(6)} %select_n.99, s32[]{:T(128)S(6)} %select_n.103, s32[]{:T(128)S(6)} %select_n.101, ...), kind=kLoop, calls=%fused_computation.50 | loop fusion | bytes 786448 | tf_op jit(solution)/shard_map/dynamic_slice | solution.py:29
  21.9 3.1 %collective-permute-start = (bf16[1,6,64,128]{3,2,1,0:T(8,128)(2,1)}, bf16[1,6,64,128]{3,2,1,0:T(8,128)(2,1)}, u32[]{:S(2)}, u32[]{:S(2)}) collective-permute-start(bf16[1,6,64,128]{3,2,1,0:T(8,128)(2,1)} %get-tuple-element.13), channel_id=1, source_target_pairs={{0,2},{2,4},{4,6},{6,0},{1,3},{3,5},{5,7},{7,1},{8,10},{10,12},{12... | collective-permute-start | bytes 294920 | tf_op jit(solution)/shard_map/ppermute | solution.py:32
  25.0 2.6 %collective-permute-start.1 = (bf16[1,6,64,128]{3,2,1,0:T(8,128)(2,1)}, bf16[1,6,64,128]{3,2,1,0:T(8,128)(2,1)}, u32[]{:S(2)}, u32[]{:S(2)}) collective-permute-start(bf16[1,6,64,128]{3,2,1,0:T(8,128)(2,1)} %get-tuple-element.12), channel_id=1, source_target_pairs={{0,4},{2,6},{4,0},{6,2},{1,5},{3,7},{5,1},{7,3},{8,12},{10,14},{12... | collective-permute-start | bytes 294920 | tf_op jit(solution)/shard_map/ppermute | solution.py:32
  28.9 2.0 %fusion.20 = bf16[768,128]{1,0:T(8,128)(2,1)S(1)} fusion(bf16[2048,128]{1,0:T(8,128)(2,1)} %param.11, bf16[1,768,2048]{2,1,0:T(8,128)(2,1)S(1)} %copy-done), kind=kOutput, calls=%fused_computation.31 | convolution fusion | flops 402751488 | bytes 3866624 | tf_op jit(solution)/shard_map/dot_general | solution.py:89
  32.3 4.1 %all-to-all-start = ((bf16[4,6,64,128]{3,2,1,0:T(8,128)(2,1)}), bf16[4,6,64,128]{3,2,1,0:T(8,128)(2,1)}, u32[]{:S(2)}, u32[]{:S(2)}) async-start(bf16[4,6,64,128]{3,2,1,0:T(8,128)(2,1)} %bitcast.103), calls=%async_computation | async-start | bytes 786432 | tf_op jit(solution)/shard_map/all_to_all | solution.py:115
  47.2 4.0 %copy.59 = bf16[2048,512]{0,1:T(8,128)(2,1)} copy(bf16[2048,512]{1,0:T(8,128)(2,1)} %param.9) | data formatting | bytes 4194304 | tf_op args[1]
  51.1 3.5 %fusion.11 = f32[768,8,64]{0,2,1:T(8,128)S(1)} fusion(bf16[8,64,2048]{2,1,0:T(8,128)(2,1)} %bitcast.101, bf16[1,768,2048]{2,1,0:T(8,128)(2,1)S(1)} %copy-done), kind=kOutput, calls=%fused_computation.21 | convolution fusion | flops 1610612736 | bytes 6815744 | tf_op jit(solution)/shard_map/dot_general | solution.py:74
  55.6 2.2 %concatenate.37 = bf16[6,128,2,4,32]{1,0,4,3,2:T(8,128)(2,1)} reshape(bf16[768,8,32]{0,2,1:T(8,128)(2,1)} %get-tuple-element.7) | data formatting | bytes 786432 | tf_op jit(solution)/shard_map/concatenate | solution.py:45
  57.8 1.9 %copy.60 = bf16[6,128,2,4,32]{1,4,3,2,0:T(8,128)(2,1)} copy(bf16[6,128,2,4,32]{1,0,4,3,2:T(8,128)(2,1)} %concatenate.37) | data formatting | bytes 786432 | tf_op jit(solution)/shard_map/concatenate | solution.py:45
  60.9 1.9 %copy.61 = bf16[6,128,2,4,32]{1,4,3,2,0:T(8,128)(2,1)} copy(bf16[6,128,2,4,32]{1,0,4,3,2:T(8,128)(2,1)} %concatenate.38) | data formatting | bytes 786432 | tf_op jit(solution)/shard_map/concatenate | solution.py:45
  62.8 1.8 %copy.52 = bf16[6,128,2,64]{1,3,2,0:T(8,128)(2,1)} copy(bf16[6,128,2,64]{3,2,1,0:T(2,128)(2,1)} %reshape.311) | data formatting | bytes 393216 | tf_op jit(solution)/shard_map/reshape | solution.py:127
  69.6 1.6 %gather_fusion.4 = bf16[24,64,128]{2,1,0:T(8,128)(2,1)S(1)} fusion(bf16[24,64,128]{2,1,0:T(8,128)(2,1)} %bitcast.105, s32[1024]{0:T(1024)S(1)} %pad_clamp_fusion.1), kind=kCustom, calls=%fused_computation.4 | custom fusion | bytes 786528 | tf_op jit(solution)/shard_map/gather | solution.py:118
  72.4 2.2 %copy.58 = bf16[6,256,2,64]{1,3,2,0:T(8,128)(2,1)S(1)} copy(bf16[6,256,2,64]{3,2,1,0:T(2,128)(2,1)} %reshape.261) | data formatting | bytes 786432 | tf_op jit(solution)/shard_map/reshape | solution.py:121
  74.6 8.7 %fusion.40 = (f32[6,2,4,128]{3,2,1,0:T(4,128)}, f32[6,2,4,128,384]{3,4,2,1,0:T(8,128)}) fusion(pred[6,128,384]{1,2,0:T(8,128)(4,1)} %pad_add_fusion, bf16[6,128,2,4,32]{1,4,3,2,0:T(8,128)(2,1)} %copy.61, bf16[6,128,2,4,32]{1,4,3,2,0:T(8,128)(2,1)} %copy.60, bf16[6,128,2,32]{1,3,2,0:T(8,128)(2,1)} %get-tuple-element.19, ...), kind=kOutput, calls=%fused_computation.87 | convolution fusion | flops 314769792 | bytes 11132928 | tf_op jit(solution)/shard_map/sub | solution.py:145
  83.3 1.6 %gather_fusion.1 = bf16[24,64,128]{2,1,0:T(8,128)(2,1)S(1)} fusion(bf16[24,64,128]{2,1,0:T(8,128)(2,1)} %bitcast.4, s32[1024]{0:T(1024)S(1)} %pad_clamp_fusion.1), kind=kCustom, calls=%fused_computation.1 | custom fusion | bytes 786528 | tf_op jit(solution)/shard_map/gather | solution.py:119
  86.2 2.2 %copy.51 = bf16[6,256,2,64]{1,3,2,0:T(8,128)(2,1)S(1)} copy(bf16[6,256,2,64]{3,2,1,0:T(2,128)(2,1)} %reshape.259) | data formatting | bytes 786432 | tf_op jit(solution)/shard_map/reshape | solution.py:122
  88.4 4.8 %fusion.19 = bf16[6,128,2,4,64]{1,4,3,2,0:T(8,128)(2,1)S(1)} fusion(f32[6,2,4,128,384]{3,4,2,1,0:T(8,128)} %get-tuple-element.18, f32[6,2,4,128]{3,2,1,0:T(4,128)} %get-tuple-element.17, bf16[6,128,2,64]{1,3,2,0:T(8,128)(2,1)} %copy.52, bf16[6,256,2,64]{1,3,2,0:T(8,128)(2,1)S(1)} %copy.51), kind=kOutput, calls=%fused_computation.29 | convolution fusion | flops 308281344 | bytes 10838016 | tf_op jit(solution)/shard_map/bngqk,bknd->bqngd/dot_general | solution.py:148
  93.7 3.5 %convolution_convert_fusion = bf16[768,2048]{1,0:T(8,128)(2,1)} fusion(bf16[512,2048]{1,0:T(8,128)(2,1)S(1)} %copy-done.8, bf16[64,8,6,128]{3,2,1,0:T(8,128)(2,1)S(1)} %bitcast.106), kind=kOutput, calls=%fused_computation.17 | convolution fusion | flops 1612185600 | bytes 6029312 | tf_op jit(solution)/shard_map/dot_general | solution.py:152
  97.3 12.3 %reduce-scatter.2.cloned.1.call-done = bf16[768,1024]{1,0:T(8,128)(2,1)} async-done(((bf16[768,2048]{1,0:T(8,128)(2,1)}), bf16[768,1024]{1,0:T(8,128)(2,1)}) %reduce-scatter.2.cloned.1.call-update) | async-done | bytes 1572880 | tf_op jit(solution)/shard_map/reduce_scatter | solution.py:153
  109.6 1.8 %fusion.8 = f32[768]{0:T(1024)S(1)} fusion(bf16[768,1024]{1,0:T(8,128)(2,1)} %reduce-scatter.2.cloned.1.call-done), kind=kLoop, calls=%fused_computation.18 | loop fusion | flops 2358528 | bytes 1575936 | tf_op jit(solution)/shard_map/reduce_sum | solution.py:156
  111.4 2.5 %psum.7 = f32[768]{0:T(1024)S(1)} all-reduce(f32[768]{0:T(1024)S(1)} %fusion.8), channel_id=1, replica_groups=mesh['dp'=4,'kv'=4,'tp'=2] {'tp'}, use_global_device_ids=true, to_apply=%region_7.8 | all-reduce | flops 768 | bytes 6144 | tf_op jit(solution)/shard_map/psum | solution.py:156
  113.9 3.0 %fusion.17 = bf16[1,768,1024]{2,1,0:T(8,128)(2,1)} fusion(bf16[768,1024]{1,0:T(8,128)(2,1)} %reduce-scatter.2.cloned.1.call-done, f32[1024]{0:T(1024)S(1)} %copy-done.7, f32[768]{0:T(1024)S(1)} %add_rsqrt_fusion), kind=kLoop, calls=%fused_computation.27 | loop fusion | flops 3145728 | bytes 3152896 | tf_op jit(solution)/shard_map/broadcast_in_dim | solution.py:159
  (77 shorter events, 32.4 us)
Async XLA Ops:
  6.5 3.4 %copy-start = (bf16[1,768,2048]{2,1,0:T(8,128)(2,1)S(1)}, bf16[1,768,2048]{2,1,0:T(8,128)(2,1)}, u32[]{:S(2)}) copy-start(bf16[1,768,2048]{2,1,0:T(8,128)(2,1)} %param.8) | copy-start | bytes 9437188
  9.9 2.3 %copy-start.1 = (f32[768,32]{0,1:T(8,128)}, f32[768,32]{0,1:T(8,128)S(1)}, u32[]{:S(2)}) copy-start(f32[768,32]{0,1:T(8,128)S(1)} %get-tuple-element.15) | copy-start | bytes 294916
  9.9 2.3 %copy-start.3 = (f32[768,32]{0,1:T(8,128)}, f32[768,32]{0,1:T(8,128)S(1)}, u32[]{:S(2)}) copy-start(f32[768,32]{0,1:T(8,128)S(1)} %get-tuple-element.16) | copy-start | bytes 294916
  9.9 4.7 %copy-start.5 = (s32[1,24,4]{1,2,0:T(4,128)S(1)}, s32[1,24,4]{1,2,0:T(4,128)}, u32[]{:S(2)}) copy-start(s32[1,24,4]{1,2,0:T(4,128)} %param.14) | copy-start | bytes 1156
  21.9 45.1 %collective-permute-start = (bf16[1,6,64,128]{3,2,1,0:T(8,128)(2,1)}, bf16[1,6,64,128]{3,2,1,0:T(8,128)(2,1)}, u32[]{:S(2)}, u32[]{:S(2)}) collective-permute-start(bf16[1,6,64,128]{3,2,1,0:T(8,128)(2,1)} %get-tuple-element.13), channel_id=1, source_target_pairs={{0,2},{2,4},{4,6},{6,0},{1,3},{3,5},{5,7},{7,1},{8,10},{10,12},{12... | collective-permute-start | bytes 294920 | tf_op jit(solution)/shard_map/ppermute | solution.py:32
  25.0 42.0 %collective-permute-start.1 = (bf16[1,6,64,128]{3,2,1,0:T(8,128)(2,1)}, bf16[1,6,64,128]{3,2,1,0:T(8,128)(2,1)}, u32[]{:S(2)}, u32[]{:S(2)}) collective-permute-start(bf16[1,6,64,128]{3,2,1,0:T(8,128)(2,1)} %get-tuple-element.12), channel_id=1, source_target_pairs={{0,4},{2,6},{4,0},{6,2},{1,5},{3,7},{5,1},{7,3},{8,12},{10,14},{12... | collective-permute-start | bytes 294920 | tf_op jit(solution)/shard_map/ppermute | solution.py:32
  27.6 9.7 %copy-start.6 = (s32[1,24,4]{1,2,0:T(4,128)S(1)}, s32[1,24,4]{1,2,0:T(4,128)}, u32[]{:S(2)}) copy-start(s32[1,24,4]{1,2,0:T(4,128)} %param.14) | copy-start | bytes 1156
  27.6 39.5 %collective-permute-start.2 = (bf16[1,6,64,128]{3,2,1,0:T(8,128)(2,1)}, bf16[1,6,64,128]{3,2,1,0:T(8,128)(2,1)}, u32[]{:S(2)}, u32[]{:S(2)}) collective-permute-start(bf16[1,6,64,128]{3,2,1,0:T(8,128)(2,1)} %get-tuple-element.14), channel_id=1, source_target_pairs={{0,6},{2,0},{4,2},{6,4},{1,7},{3,1},{5,3},{7,5},{8,14},{10,8},{12,... | collective-permute-start | bytes 294920 | tf_op jit(solution)/shard_map/ppermute | solution.py:32
  32.3 51.0 %all-to-all-start = ((bf16[4,6,64,128]{3,2,1,0:T(8,128)(2,1)}), bf16[4,6,64,128]{3,2,1,0:T(8,128)(2,1)}, u32[]{:S(2)}, u32[]{:S(2)}) async-start(bf16[4,6,64,128]{3,2,1,0:T(8,128)(2,1)} %bitcast.103), calls=%async_computation | async-start | bytes 786432 | tf_op jit(solution)/shard_map/all_to_all | solution.py:115
  36.4 73.2 %reduce-scatter.2.cloned.1.call-start = ((), (), s32[]{:S(2)}) async-start(), calls=%async_computation.2 | async-start | bytes 4718592 | tf_op jit(solution)/shard_map/reduce_scatter | solution.py:153
  51.1 3.5 %copy-start.2 = (f32[768,32]{0,1:T(8,128)S(1)}, f32[768,32]{0,1:T(8,128)}, u32[]{:S(2)}) copy-start(f32[768,32]{0,1:T(8,128)} %copy-done.1) | copy-start | bytes 294916
  51.1 3.5 %copy-start.4 = (f32[768,32]{0,1:T(8,128)S(1)}, f32[768,32]{0,1:T(8,128)}, u32[]{:S(2)}) copy-start(f32[768,32]{0,1:T(8,128)} %copy-done.3) | copy-start | bytes 294916
  88.4 5.4 %copy-start.8 = (bf16[512,2048]{1,0:T(8,128)(2,1)S(1)}, bf16[512,2048]{1,0:T(8,128)(2,1)}, u32[]{:S(2)}) copy-start(bf16[512,2048]{1,0:T(8,128)(2,1)} %param.12) | copy-start | bytes 6291460
  97.3 16.6 %copy-start.7 = (f32[1024]{0:T(1024)S(1)}, f32[1024]{0:T(1024)}, u32[]{:S(2)}) copy-start(f32[1024]{0:T(1024)} %param.13) | copy-start | bytes 12292
Sparse Core Ops, SparseCore 0:
  97.4 12.1 reduce-scatter.1
